TPU v7x, 32 devices: a whole 2x2x4 slice. The times are simulated.
32 devices in a mesh: sp: 8 (over z, x), dp: 4 (over y, core).
Axes of the slice: x: 2, y: 2, z: 4, core: 2. Of those that a mesh axis runs over, the one named last changes fastest.
Arguments:
- skip_stream_entering: bfloat16 [4, 1024, 2048], P('dp', 'sp'), may hold values from -6 to 6
- mapped_probe_matrix: bfloat16 [4, 1024, 2048], P('dp', 'sp'), may hold values from -6 to 6
- mapped_lookup_matrix: bfloat16 [4, 1024, 2048], P('dp', 'sp'), may hold values from -6 to 6
- mapped_content_matrix: bfloat16 [4, 1024, 4096], P('dp', 'sp'), may hold values from -6 to 6
- retention_preactivation: bfloat16 [4, 1024, 2048], P('dp', 'sp'), may hold values from -4 to 12
- extra_shrinkage: float32 [4, 16, 1024], P('dp', 'sp'), may hold values from -0.6932 to 0
- attention_group_scale: float32 [4096], replicated, may hold values from 0.1 to 1.9
- final_projection_matrix: bfloat16 [4096, 2048], P(None, 'dp'), may hold values from -0.09375 to 0.09375
- blender_branch_scale: float32 [2048], replicated, may hold values from 0.1 to 1.9
- specialist_prenormal_scale: float32 [2048], replicated, may hold values from 0.1 to 1.9
- specialist_switch_matrix: bfloat16 [32, 2048, 1024], P(('sp', 'dp')), may hold values from -0.125 to 0.125
- specialist_expand_matrix: bfloat16 [32, 2048, 1024], P(('sp', 'dp')), may hold values from -0.125 to 0.125
- specialist_contract_matrix: bfloat16 [32, 1024, 2048], P(('sp', 'dp')), may hold values from -0.1875 to 0.1875
- specialist_branch_scale: float32 [2048], replicated, may hold values from 0.1 to 1.9
- assigned_specialists: int32 [4, 1024, 2], P('dp', 'sp'), may hold values from 0 to 31, all different within a row; in each aligned block of 128 rows (0 to 127, 128 to 255, ..., all dimensions but the last counted through in order) at most 13 rows name the same one
- dispatcher_logits: float32 [4, 1024, 2], P('dp', 'sp'), may hold values from 0.2 to 1
Outputs:
- layer_out: bfloat16 [4, 1024, 2048], P('dp', 'sp')
Inputs may be any that keep to these rules, and one draw needn't show every extreme that they name: `assigned_specialists`: in the rows of one device no expert is named more than 13 times; in every draw some expert reaches 13 on some device.
All inputs are finite; a program needn't handle non-finite values.
Results may differ from a plain program's by a relative error of at most 0.013.
Values may be sent and summed in bfloat16 or wider, within the bound.
A program may use at most 128 MiB of HBM per device.

v0:
```python
import jax
import jax.numpy as jnp
from jax import lax
from jax.sharding import PartitionSpec as P

D = 2048
ATTENTION_GROUPS = 16
KEY_WIDTH = 128
DV = 256
TOP = 2
BLOCK = 64
epsilon = 1e-06
softness_factor = 16.0
highest = lax.Precision.HIGHEST


def rms_scale(values, gain):
    mean_square = jnp.mean(values * values, axis=-1, keepdims=True)
    return values * lax.rsqrt(mean_square + epsilon) * gain


def combine_states(earlier, later):
    return (earlier[0] * later[0], later[0][..., None] * earlier[1] + later[1])


def block_attention(query_f, key_f, value_f, shrink_exponent):
    length_value, head_count, key_dim = query_f.shape
    value_dim = value_f.shape[-1]
    block_count = length_value // BLOCK
    query_blocks = query_f.reshape(block_count, BLOCK, head_count, key_dim)
    key_blocks = key_f.reshape(block_count, BLOCK, head_count, key_dim)
    value_blocks = value_f.reshape(block_count, BLOCK, head_count, value_dim)
    within = jnp.cumsum(shrink_exponent.reshape(block_count, BLOCK, head_count, key_dim), axis=1)
    block_end = within[:, -1]
    lifted = query_blocks * jnp.exp(within)
    lowered = key_blocks * jnp.exp(-within)
    scores = jnp.einsum("nthk,nshk->nhts", lifted, lowered, precision=highest)
    causal = jnp.arange(BLOCK)[:, None] >= jnp.arange(BLOCK)[None, :]
    scores = jnp.where(causal, scores, 0.0)
    inside = jnp.einsum("nhts,nshv->nthv", scores, value_blocks, precision=highest)
    carried_keys = key_blocks * jnp.exp(block_end[:, None] - within)
    updates = jnp.einsum("nshk,nshv->nhkv", carried_keys, value_blocks, precision=highest)
    decays = jnp.exp(block_end)
    total_decay, states = lax.associative_scan(combine_states, (decays, updates), axis=0)
    entering = jnp.concatenate([jnp.zeros_like(states[:1]), states[:-1]], axis=0)
    across = jnp.einsum("nthk,nhkv->nthv", lifted, entering, precision=highest)
    outputs = (inside + across).reshape(length_value, head_count, value_dim)
    offsets = jnp.cumsum(block_end, axis=0) - block_end
    reached = (query_blocks * jnp.exp(within + offsets[:, None])).reshape(
        length_value, head_count, key_dim
    )
    return (outputs, total_decay[-1], states[-1], reached)


def shards(
    skip_stream_entering,
    mapped_probe_matrix,
    mapped_lookup_matrix,
    mapped_content_matrix,
    retention_preactivation,
    extra_shrinkage,
    attention_group_scale,
    final_projection_matrix,
    blender_branch_scale,
    specialist_prenormal_scale,
    specialist_switch_matrix,
    specialist_expand_matrix,
    specialist_contract_matrix,
    specialist_branch_scale,
    assigned_specialists,
    dispatcher_logits,
):
    tok_rows = mapped_probe_matrix.shape[1]
    sp_count = lax.axis_size("sp")
    dp_count = lax.axis_size("dp")
    query_local = mapped_probe_matrix[0].reshape(tok_rows, ATTENTION_GROUPS, KEY_WIDTH)
    key_local = mapped_lookup_matrix[0].reshape(tok_rows, ATTENTION_GROUPS, KEY_WIDTH)
    value_local = mapped_content_matrix[0].reshape(tok_rows, ATTENTION_GROUPS, DV)
    decay_local = retention_preactivation[0].reshape(tok_rows, ATTENTION_GROUPS, KEY_WIDTH)
    arrived = (
        lax.all_to_all(query_local, "sp", split_axis=1, concat_axis=0, tiled=True),
        lax.all_to_all(key_local, "sp", split_axis=1, concat_axis=0, tiled=True),
        lax.all_to_all(value_local, "sp", split_axis=1, concat_axis=0, tiled=True),
        lax.all_to_all(decay_local, "sp", split_axis=1, concat_axis=0, tiled=True),
    )
    query_head, key_head, value_head, head_decay = arrived
    own_heads = query_head.shape[1]
    shrink_exponent = jax.nn.log_sigmoid(head_decay.astype(jnp.float32)) / softness_factor
    shrink_exponent = shrink_exponent + jnp.transpose(extra_shrinkage[0])[:, :, None]
    outputs = block_attention(
        query_head.astype(jnp.float32) * KEY_WIDTH ** (-0.5),
        key_head.astype(jnp.float32),
        value_head.astype(jnp.float32),
        shrink_exponent,
    )[0]
    offset = lax.axis_index("sp") * (own_heads * DV)
    gains = lax.dynamic_slice_in_dim(attention_group_scale, offset, own_heads * DV).reshape(
        own_heads, DV
    )
    normed = rms_scale(outputs, gains).astype(jnp.bfloat16)
    attention_group_result = lax.all_to_all(normed, "sp", split_axis=0, concat_axis=1, tiled=True)
    flat_heads = attention_group_result.reshape(tok_rows, ATTENTION_GROUPS * DV)
    projected = jnp.dot(
        flat_heads,
        lax.all_gather(final_projection_matrix, "dp", axis=1, tiled=True),
        preferred_element_type=jnp.float32,
    ).astype(jnp.bfloat16)
    stream = skip_stream_entering[0].astype(jnp.float32)
    residual = (stream + rms_scale(projected.astype(jnp.float32), blender_branch_scale)).astype(
        jnp.bfloat16
    )
    expert_in = rms_scale(residual.astype(jnp.float32), specialist_prenormal_scale).astype(
        jnp.bfloat16
    )
    expert_total = sp_count * dp_count
    capacity = max(2, 5 * tok_rows * TOP // (3 * expert_total))
    chosen = assigned_specialists[0].reshape(-1)
    pair_total = chosen.shape[0]
    onehot = (chosen[:, None] == jnp.arange(expert_total, dtype=jnp.int32)[None, :]).astype(
        jnp.int32
    )
    ranks = jnp.sum((jnp.cumsum(onehot, axis=0) - onehot) * onehot, axis=1)
    slots = chosen * capacity + ranks
    table = jnp.full((expert_total * capacity,), pair_total, jnp.int32)
    table = table.at[slots].set(jnp.arange(pair_total, dtype=jnp.int32))
    padded = jnp.concatenate([expert_in, jnp.zeros((1, D), jnp.bfloat16)], axis=0)
    outgoing = padded[table // TOP].reshape(expert_total, capacity, D)
    arrived_rows = lax.all_to_all(outgoing, ("sp", "dp"), split_axis=0, concat_axis=0, tiled=True)
    row_block = arrived_rows.reshape(-1, D)
    gate_part = jnp.dot(row_block, specialist_switch_matrix[0], preferred_element_type=jnp.float32)
    up_part = jnp.dot(row_block, specialist_expand_matrix[0], preferred_element_type=jnp.float32)
    hidden_units = (jax.nn.silu(gate_part) * up_part).astype(jnp.bfloat16)
    result = jnp.dot(
        hidden_units, specialist_contract_matrix[0], preferred_element_type=jnp.float32
    )
    returned = lax.all_to_all(
        result.astype(jnp.bfloat16).reshape(arrived_rows.shape),
        ("sp", "dp"),
        split_axis=0,
        concat_axis=0,
        tiled=True,
    )
    flat_back = returned.reshape(expert_total * capacity, D)
    pair_rows = flat_back[slots].reshape(tok_rows, TOP, D)
    weights = dispatcher_logits[0]
    weights = weights / jnp.sum(weights, axis=1, keepdims=True)
    combined = jnp.sum(pair_rows.astype(jnp.float32) * weights[:, :, None], axis=1)
    layer_out = residual.astype(jnp.float32) + rms_scale(combined, specialist_branch_scale)
    return layer_out.astype(jnp.bfloat16)[None]


def solution(mesh):
    return jax.shard_map(
        shards,
        mesh=mesh,
        in_specs=(
            P("dp", "sp", None),
            P("dp", "sp", None),
            P("dp", "sp", None),
            P("dp", "sp", None),
            P("dp", "sp", None),
            P("dp", "sp", None),
            P(),
            P(None, "dp"),
            P(),
            P(),
            P(("sp", "dp"), None, None),
            P(("sp", "dp"), None, None),
            P(("sp", "dp"), None, None),
            P(),
            P("dp", "sp", None),
            P("dp", "sp", None),
        ),
        out_specs=P("dp", "sp", None),
        check_vma=False,
    )
```

profile of v0, /device:TPU:0, one launch (start us, length us, event | category | flops | bytes accessed | tf_op | source)
XLA Modules:
  0.0 359.1 jit_solution(7891554783984080326)
XLA Ops:
  8.6 7.3 %all-to-all-start.1 = ((bf16[128,16,128]{0,2,1:T(8,128)(2,1)}), bf16[128,16,128]{0,2,1:T(8,128)(2,1)S(1)}, u32[]{:S(2)}, u32[]{:S(2)}) async-start(bf16[128,16,128]{0,2,1:T(8,128)(2,1)} %bitcast.6), calls=%async_computation.1 | async-start | bytes 1048576 | tf_op jit(solution)/shard_map/all_to_all | solution.py:84
  16.9 13.4 %all-to-all-done.1 = bf16[128,16,128]{0,2,1:T(8,128)(2,1)S(1)} async-done(((bf16[128,16,128]{0,2,1:T(8,128)(2,1)}), bf16[128,16,128]{0,2,1:T(8,128)(2,1)S(1)}, u32[]{:S(2)}, u32[]{:S(2)}) %all-to-all-start.1) | async-done | bytes 524320 | tf_op jit(solution)/shard_map/all_to_all | solution.py:84
  30.3 3.6 %all-to-all-start.2 = ((bf16[128,16,128]{0,2,1:T(8,128)(2,1)}), bf16[128,16,128]{0,2,1:T(8,128)(2,1)S(1)}, u32[]{:S(2)}, u32[]{:S(2)}) async-start(bf16[128,16,128]{0,2,1:T(8,128)(2,1)} %bitcast.13), calls=%async_computation.2 | async-start | bytes 1048576 | tf_op jit(solution)/shard_map/all_to_all | solution.py:82
  35.0 13.7 %all-to-all-done.2 = bf16[128,16,128]{0,2,1:T(8,128)(2,1)S(1)} async-done(((bf16[128,16,128]{0,2,1:T(8,128)(2,1)}), bf16[128,16,128]{0,2,1:T(8,128)(2,1)S(1)}, u32[]{:S(2)}, u32[]{:S(2)}) %all-to-all-start.2) | async-done | bytes 524320 | tf_op jit(solution)/shard_map/all_to_all | solution.py:82
  48.7 4.2 %all-to-all-start = ((bf16[128,16,128]{0,2,1:T(8,128)(2,1)}), bf16[128,16,128]{0,2,1:T(8,128)(2,1)}, u32[]{:S(2)}, u32[]{:S(2)}) async-start(bf16[128,16,128]{0,2,1:T(8,128)(2,1)} %bitcast.1), calls=%async_computation | async-start | bytes 1048576 | tf_op jit(solution)/shard_map/all_to_all | solution.py:81
  56.1 11.0 %all-to-all-done = bf16[128,16,128]{0,2,1:T(8,128)(2,1)} async-done(((bf16[128,16,128]{0,2,1:T(8,128)(2,1)}), bf16[128,16,128]{0,2,1:T(8,128)(2,1)}, u32[]{:S(2)}, u32[]{:S(2)}) %all-to-all-start) | async-done | bytes 524320 | tf_op jit(solution)/shard_map/all_to_all | solution.py:81
  67.1 3.7 %all-to-all-start.3 = ((bf16[128,16,256]{0,2,1:T(8,128)(2,1)}), bf16[128,16,256]{0,2,1:T(8,128)(2,1)S(1)}, u32[]{:S(2)}, u32[]{:S(2)}) async-start(bf16[128,16,256]{0,2,1:T(8,128)(2,1)} %bitcast.18), calls=%async_computation.3 | async-start | bytes 2097152 | tf_op jit(solution)/shard_map/all_to_all | solution.py:83
  76.7 4.0 %exponential_multiply_fusion = (f32[16,64,2,128]{3,0,1,2:T(8,128)}, f32[16,64,2,128]{3,0,1,2:T(8,128)S(1)}, f32[16,64,2,128]{3,0,1,2:T(8,128)S(1)}) fusion(f32[16,64,2,128]{3,0,1,2:T(8,128)S(1)} %fusion.30, f32[16,64,2,128]{3,1,0,2:T(8,128)} %bitcast.106, f32[16,2,128]{2,0,1:T(8,128)S(1)} %slice_bitcast_fusion, f32[16,64,2,128]{3,1,0,2:T(8,128)} %bitcast.107), kind=kLoop, calls=%fused_computation.49 | loop fusion | flops 1310720 | bytes 6307840 | tf_op jit(solution)/shard_map/mul | solution.py:41
  80.7 3.5 convolution_select_fusion
  84.2 12.4 %all-to-all-done.3 = bf16[128,16,256]{0,2,1:T(8,128)(2,1)S(1)} async-done(((bf16[128,16,256]{0,2,1:T(8,128)(2,1)}), bf16[128,16,256]{0,2,1:T(8,128)(2,1)S(1)}, u32[]{:S(2)}, u32[]{:S(2)}) %all-to-all-start.3) | async-done | bytes 1048608 | tf_op jit(solution)/shard_map/all_to_all | solution.py:83
  97.1 3.7 %fusion.27 = f32[16,2,128,256]{3,2,1,0:T(8,128)S(1)} fusion(f32[16,64,2,128]{3,0,1,2:T(8,128)} %get-tuple-element.7, bf16[16,64,2,256]{3,1,0,2:T(8,128)(2,1)S(1)} %bitcast.97), kind=kOutput, calls=%fused_computation.40 | convolution fusion | flops 805306368 | bytes 6291456 | tf_op jit(solution)/shard_map/nshk,nshv->nhkv/dot_general | solution.py:42
  106.4 4.2 %pad.30 = f32[4,2,128,256]{3,2,1,0:T(8,128)} pad(f32[2,2,128,256]{3,2,1,0:T(8,128)} %pad_add_fusion, f32[]{:T(128)} %constant.27.clone.1), padding=1_0_1x0_0_0x0_0_0x0_0_0 | pad | bytes 1572868 | tf_op jit(solution)/shard_map/pad | solution.py:44
  112.6 4.1 %pad.29 = f32[4,2,128,256]{3,2,1,0:T(8,128)} pad(f32[2,2,128,256]{3,2,1,0:T(8,128)} %pad_maximum_fusion.2, f32[]{:T(128)} %constant.27.clone.1), padding=0_1_1x0_0_0x0_0_0x0_0_0 | pad | bytes 1572868 | tf_op jit(solution)/shard_map/pad | solution.py:44
  116.7 2.8 add.160
  121.5 3.9 %pad.31 = f32[8,2,128,256]{3,2,1,0:T(8,128)S(1)} pad(f32[4,2,128,256]{3,2,1,0:T(8,128)} %pad_maximum_fusion.1, f32[]{:T(128)} %constant.27.clone.1), padding=0_1_1x0_0_0x0_0_0x0_0_0 | pad | bytes 3145732 | tf_op jit(solution)/shard_map/pad | solution.py:44
  125.4 6.6 %pad.32 = f32[8,2,128,256]{3,2,1,0:T(8,128)} pad(f32[4,2,128,256]{3,2,1,0:T(8,128)} %add.160, f32[]{:T(128)} %constant.27.clone.1), padding=1_0_1x0_0_0x0_0_0x0_0_0 | pad | bytes 3145732 | tf_op jit(solution)/shard_map/pad | solution.py:44
  132.0 3.2 add.162
  135.2 11.5 %pad.66 = f32[16,2,128,256]{3,2,1,0:T(8,128)} pad(f32[8,2,128,256]{3,2,1,0:T(8,128)} %add.162, f32[]{:T(128)} %constant.27.clone.1), padding=1_0_1x0_0_0x0_0_0x0_0_0 | pad | bytes 6291460
  150.6 11.5 %pad.44 = f32[15,2,128,256]{3,2,1,0:T(8,128)} pad(f32[8,2,128,256]{3,2,1,0:T(8,128)} %pad_maximum_fusion, f32[]{:T(128)} %constant.27.clone.1), padding=0_0_1x0_0_0x0_0_0x0_0_0 | pad | bytes 6029316 | tf_op jit(solution)/shard_map/slice | solution.py:45
  164.3 2.9 fusion.16.clone.4
  167.2 2.9 multiply_reduce_fusion.1
  172.7 3.6 %all-to-all-start.4 = ((bf16[1024,2,256]{2,1,0:T(2,128)(2,1)}), bf16[1024,2,256]{2,1,0:T(2,128)(2,1)S(1)}, u32[]{:S(2)}, u32[]{:S(2)}) async-start(bf16[1024,2,256]{2,1,0:T(2,128)(2,1)} %copy.206), calls=%async_computation.4 | async-start | bytes 2097152 | tf_op jit(solution)/shard_map/all_to_all | solution.py:101
  179.4 22.9 %all-to-all-done.4 = bf16[1024,2,256]{2,1,0:T(2,128)(2,1)S(1)} async-done(((bf16[1024,2,256]{2,1,0:T(2,128)(2,1)}), bf16[1024,2,256]{2,1,0:T(2,128)(2,1)S(1)}, u32[]{:S(2)}, u32[]{:S(2)}) %all-to-all-start.4) | async-done | bytes 1048608 | tf_op jit(solution)/shard_map/all_to_all | solution.py:101
  203.5 8.3 %multiply_reduce_fusion.3 = (f32[128]{0:T(128)S(1)}, f32[128,2048]{1,0:T(8,128)S(1)}) fusion(bf16[128,4096]{0,1:T(8,128)(2,1)S(1)} %bitcast.99, bf16[4096,2048]{1,0:T(8,128)(2,1)} %all-gather.2.cloned.1.call-done), kind=kOutput, calls=%fused_computation.47 | convolution fusion | flops 2148532224 | bytes 18874880 | tf_op jit(solution)/shard_map/dot_general | solution.py:103
  212.7 3.2 gather_fusion
  217.6 52.3 %all_to_all.67 = bf16[32,13,2048]{2,1,0:T(8,128)(2,1)} all-to-all(bf16[32,13,2048]{2,1,0:T(8,128)(2,1)S(1)} %reshape.176), channel_id=1, replica_groups=mesh['sp'=8,'dp'=4] {'sp','dp'}, dimensions={0} | all-to-all | bytes 3407872 | tf_op jit(solution)/shard_map/all_to_all | solution.py:128
  271.8 5.3 %fusion.4 = f32[416,1024]{1,0:T(8,128)} fusion(bf16[416,2048]{1,0:T(8,128)(2,1)S(1)} %reshape.177, bf16[1,2048,1024]{2,1,0:T(8,128)(2,1)} %param.26), kind=kOutput, calls=%fused_computation.7 | convolution fusion | flops 1744830464 | bytes 7602176 | tf_op jit(solution)/shard_map/dot_general | solution.py:130
  277.1 8.9 %fusion.8 = bf16[416,2048]{1,0:T(8,128)(2,1)} fusion(bf16[1,1024,2048]{2,1,0:T(8,128)(2,1)} %param.28, f32[416,1024]{1,0:T(8,128)} %fusion.4, bf16[416,2048]{1,0:T(8,128)(2,1)S(1)} %reshape.177, bf16[1,2048,1024]{2,1,0:T(8,128)(2,1)} %param.27), kind=kOutput, calls=%fused_computation.12 | convolution fusion | flops 3493068800 | bytes 13500416 | tf_op jit(solution)/shard_map/dot_general | solution.py:133
  286.0 2.8 reshape.178
  288.8 4.1 %all-to-all-start.6 = ((bf16[32,13,2048]{2,1,0:T(8,128)(2,1)}), bf16[32,13,2048]{2,1,0:T(8,128)(2,1)}, u32[]{:S(2)}, u32[]{:S(2)}) async-start(bf16[32,13,2048]{2,1,0:T(8,128)(2,1)} %reshape.178), calls=%async_computation.6 | async-start | bytes 4194304 | tf_op jit(solution)/shard_map/all_to_all | solution.py:136
  293.1 48.2 %all-to-all-done.6 = bf16[32,13,2048]{2,1,0:T(8,128)(2,1)} async-done(((bf16[32,13,2048]{2,1,0:T(8,128)(2,1)}), bf16[32,13,2048]{2,1,0:T(8,128)(2,1)}, u32[]{:S(2)}, u32[]{:S(2)}) %all-to-all-start.6) | async-done | bytes 1703968 | tf_op jit(solution)/shard_map/all_to_all | solution.py:136
  347.9 3.2 multiply_reduce_fusion
  (139 shorter events, 48.5 us)
Async XLA Ops:
  6.5 1.0 copy-start.12
  6.5 196.9 %all-gather.2.cloned.1.call-start = ((), (), s32[]{:S(2)}) async-start(), calls=%async_computation.7 | async-start | bytes 20971520 | tf_op jit(solution)/shard_map/all_gather | solution.py:105
  7.6 8.3 %copy-start.13 = (bf16[1,128,2048]{2,1,0:T(8,128)(2,1)S(1)}, bf16[1,128,2048]{2,1,0:T(8,128)(2,1)}, u32[]{:S(2)}) copy-start(bf16[1,128,2048]{2,1,0:T(8,128)(2,1)} %param.18) | copy-start | bytes 1572868
  7.6 26.4 %copy-start.14 = (bf16[1,128,2048]{2,1,0:T(8,128)(2,1)S(1)}, bf16[1,128,2048]{2,1,0:T(8,128)(2,1)}, u32[]{:S(2)}) copy-start(bf16[1,128,2048]{2,1,0:T(8,128)(2,1)} %param.17) | copy-start | bytes 1572868
  8.6 21.8 %all-to-all-start.1 = ((bf16[128,16,128]{0,2,1:T(8,128)(2,1)}), bf16[128,16,128]{0,2,1:T(8,128)(2,1)S(1)}, u32[]{:S(2)}, u32[]{:S(2)}) async-start(bf16[128,16,128]{0,2,1:T(8,128)(2,1)} %bitcast.6), calls=%async_computation.1 | async-start | bytes 1048576 | tf_op jit(solution)/shard_map/all_to_all | solution.py:84
  15.9 37.0 %copy-start.19 = (f32[1,2,1024]{2,1,0:T(2,128)S(1)}, f32[1,2,1024]{2,1,0:T(2,128)}, u32[]{:S(2)}) copy-start(f32[1,2,1024]{2,1,0:T(2,128)} %param.21) | copy-start | bytes 24580
  15.9 37.0 %copy-start.10 = (bf16[1,128,4096]{2,1,0:T(8,128)(2,1)S(1)}, bf16[1,128,4096]{2,1,0:T(8,128)(2,1)}, u32[]{:S(2)}) copy-start(bf16[1,128,4096]{2,1,0:T(8,128)(2,1)} %param.19) | copy-start | bytes 3145732
  30.3 18.3 %all-to-all-start.2 = ((bf16[128,16,128]{0,2,1:T(8,128)(2,1)}), bf16[128,16,128]{0,2,1:T(8,128)(2,1)S(1)}, u32[]{:S(2)}, u32[]{:S(2)}) async-start(bf16[128,16,128]{0,2,1:T(8,128)(2,1)} %bitcast.13), calls=%async_computation.2 | async-start | bytes 1048576 | tf_op jit(solution)/shard_map/all_to_all | solution.py:82
  48.7 6.5 %copy-start.9 = (bf16[128,16,128]{0,2,1:T(8,128)(2,1)}, bf16[128,16,128]{0,2,1:T(8,128)(2,1)S(1)}, u32[]{:S(2)}) copy-start(bf16[128,16,128]{0,2,1:T(8,128)(2,1)S(1)} %all-to-all-done.2) | copy-start | bytes 1572868
  48.7 18.4 %all-to-all-start = ((bf16[128,16,128]{0,2,1:T(8,128)(2,1)}), bf16[128,16,128]{0,2,1:T(8,128)(2,1)}, u32[]{:S(2)}, u32[]{:S(2)}) async-start(bf16[128,16,128]{0,2,1:T(8,128)(2,1)} %bitcast.1), calls=%async_computation | async-start | bytes 1048576 | tf_op jit(solution)/shard_map/all_to_all | solution.py:81
  67.1 29.5 %all-to-all-start.3 = ((bf16[128,16,256]{0,2,1:T(8,128)(2,1)}), bf16[128,16,256]{0,2,1:T(8,128)(2,1)S(1)}, u32[]{:S(2)}, u32[]{:S(2)}) async-start(bf16[128,16,256]{0,2,1:T(8,128)(2,1)} %bitcast.18), calls=%async_computation.3 | async-start | bytes 2097152 | tf_op jit(solution)/shard_map/all_to_all | solution.py:83
  97.1 3.7 %copy-start.2 = (bf16[8,128,2,256]{3,1,0,2:T(8,128)(2,1)}, bf16[8,128,2,256]{3,1,0,2:T(8,128)(2,1)S(1)}, u32[]{:S(2)}) copy-start(bf16[8,128,2,256]{3,1,0,2:T(8,128)(2,1)S(1)} %copy.193) | copy-start | bytes 3145732
  100.8 1.9 copy-start
  103.7 1.0 copy-start.6
  104.9 0.7 copy-start.8
  116.7 2.8 copy-start.4
  116.7 2.8 copy-start.5
  119.5 1.0 copy-start.11
  146.6 2.5 slice-start
  150.6 11.5 %copy-start.3 = (bf16[8,128,2,256]{3,1,0,2:T(8,128)(2,1)S(1)}, bf16[8,128,2,256]{3,1,0,2:T(8,128)(2,1)}, u32[]{:S(2)}) copy-start(bf16[8,128,2,256]{3,1,0,2:T(8,128)(2,1)} %copy-done.2) | copy-start | bytes 3145732
  150.6 11.5 %copy-start.7 = (f32[16,2,64,64]{3,2,1,0:T(8,128)S(1)}, f32[16,2,64,64]{3,2,1,0:T(8,128)}, u32[]{:S(2)}) copy-start(f32[16,2,64,64]{3,2,1,0:T(8,128)} %convolution_select_fusion) | copy-start | bytes 1572868
  162.1 2.2 copy-start.1
  170.7 5.7 %copy-start.20 = (s32[1,128,2]{1,2,0:T(2,128)S(1)}, s32[1,128,2]{1,2,0:T(2,128)}, u32[]{:S(2)}) copy-start(s32[1,128,2]{1,2,0:T(2,128)} %param.30) | copy-start | bytes 3076
  172.7 29.6 %all-to-all-start.4 = ((bf16[1024,2,256]{2,1,0:T(2,128)(2,1)}), bf16[1024,2,256]{2,1,0:T(2,128)(2,1)S(1)}, u32[]{:S(2)}, u32[]{:S(2)}) async-start(bf16[1024,2,256]{2,1,0:T(2,128)(2,1)} %copy.206), calls=%async_computation.4 | async-start | bytes 2097152 | tf_op jit(solution)/shard_map/all_to_all | solution.py:101
  203.4 8.3 %copy-start.15 = (bf16[1,128,2048]{2,1,0:T(8,128)(2,1)S(1)}, bf16[1,128,2048]{2,1,0:T(8,128)(2,1)}, u32[]{:S(2)}) copy-start(bf16[1,128,2048]{2,1,0:T(8,128)(2,1)} %param.16) | copy-start | bytes 1572868
  203.5 8.3 %copy-start.16 = (f32[2048]{0:T(1024)S(1)}, f32[2048]{0:T(1024)}, u32[]{:S(2)}) copy-start(f32[2048]{0:T(1024)} %param.24) | copy-start | bytes 24580
  211.7 0.7 copy-start.17
  288.8 4.1 %copy-start.21 = (f32[1,128,2]{1,2,0:T(2,128)S(1)}, f32[1,128,2]{1,2,0:T(2,128)}, u32[]{:S(2)}) copy-start(f32[1,128,2]{1,2,0:T(2,128)} %param.31) | copy-start | bytes 3076
  288.8 52.5 %all-to-all-start.6 = ((bf16[32,13,2048]{2,1,0:T(8,128)(2,1)}), bf16[32,13,2048]{2,1,0:T(8,128)(2,1)}, u32[]{:S(2)}, u32[]{:S(2)}) async-start(bf16[32,13,2048]{2,1,0:T(8,128)(2,1)} %reshape.178), calls=%async_computation.6 | async-start | bytes 4194304 | tf_op jit(solution)/shard_map/all_to_all | solution.py:136
  347.8 3.3 copy-start.18
Sparse Core Ops, SparseCore 0:
  8.9 108.6 all-gather.1
where the time goes:
time: 361 us; the launch traced here: 359 us
  waiting for transfers between devices  122 us (34%)
  local copies, waits for them, and re-layouts  78.8 us (22%)
  blocking collectives  52.3 us (14%)
  matrix products  33.5 us (9%)
  other arithmetic  31.6 us (9%)
  starting transfers between devices  26.5 us (7%)
  between operations  14 us (4%)
    all_to_all x1, blocking collectives, shards(): lax.all_to_all(outgoing, ('sp', 'dp'), split_axis=0, concat_axis=0, tiled...  52.3 us
    all_to_all x1, waiting for transfers between devices, shards(): lax.all_to_all(result.astype(jnp.bfloat16).reshape(arrived_rows.shape), (...  48.2 us
    all_to_all x1, waiting for transfers between devices, shards(): lax.all_to_all(normed, 'sp', split_axis=0, concat_axis=1, tiled=True)  22.9 us
    unnamed x50, local copies, waits for them, and re-layouts  21.6 us
    pad x4, local copies, waits for them, and re-layouts, block_attention(): lax.associative_scan(combine_states, (decays, updates), axis=0)  18.7 us
    all_to_all x1, waiting for transfers between devices, shards(): lax.all_to_all(key_local, 'sp', split_axis=1, concat_axis=0, tiled=True)  13.7 us
    all_to_all x1, waiting for transfers between devices, shards(): lax.all_to_all(decay_local, 'sp', split_axis=1, concat_axis=0, tiled=True)  13.4 us
    all_to_all x1, waiting for transfers between devices, shards(): lax.all_to_all(value_local, 'sp', split_axis=1, concat_axis=0, tiled=True)  12.4 us
  transfers between devices with their start and end apart: 7, of which 6 were waited for; matrix products, arithmetic and copies ran while one was open for 26% of the time, Pallas kernels for 0%

commit v1 on v0

--- a/solution.py
+++ b/solution.py
@@ -98,7 +98,10 @@
         own_heads, DV
     )
     normed = rms_scale(outputs, gains).astype(jnp.bfloat16)
-    attention_group_result = lax.all_to_all(normed, "sp", split_axis=0, concat_axis=1, tiled=True)
+    attention_group_result = jnp.concatenate(
+        lax.all_to_all(jnp.stack(jnp.split(normed, lax.axis_size("sp"), axis=0)), "sp", 0, 0),
+        axis=1,
+    )
     flat_heads = attention_group_result.reshape(tok_rows, ATTENTION_GROUPS * DV)
     projected = jnp.dot(
         flat_heads,

time: 361 us -> 364 us (level)
    unnamed x50 -> x57, local copies, waits for them, and re-layouts: 21.6 us -> 26.2 us
  transfers between devices with their start and end apart: 7 -> 7, of which waited for: 6 -> 6; matrix products, arithmetic and copies ran while one was open for 26% -> 27% of each run, Pallas kernels for 0% -> 0%
where the time goes in v1:
time: 364 us; the launch traced here: 362 us
  waiting for transfers between devices  123 us (34%)
  local copies, waits for them, and re-layouts  81.6 us (22%)
  blocking collectives  52.3 us (14%)
  matrix products  33.5 us (9%)
  other arithmetic  31.6 us (9%)
  starting transfers between devices  26.2 us (7%)
  between operations  14 us (4%)
    all_to_all x1, blocking collectives, shards(): lax.all_to_all(outgoing, ('sp', 'dp'), split_axis=0, concat_axis=0, tiled...  52.3 us
    all_to_all x1, waiting for transfers between devices, shards(): lax.all_to_all(result.astype(jnp.bfloat16).reshape(arrived_rows.shape), (...  48.5 us
    unnamed x57, local copies, waits for them, and re-layouts  26.2 us
    all_to_all x1, waiting for transfers between devices, shards(): lax.all_to_all(jnp.stack(jnp.split(normed, lax.axis_size('sp'), axis=0)),...  22.9 us
    pad x4, local copies, waits for them, and re-layouts, block_attention(): lax.associative_scan(combine_states, (decays, updates), axis=0)  18.7 us
    all_to_all x1, waiting for transfers between devices, shards(): lax.all_to_all(key_local, 'sp', split_axis=1, concat_axis=0, tiled=True)  13.7 us
    all_to_all x1, waiting for transfers between devices, shards(): lax.all_to_all(decay_local, 'sp', split_axis=1, concat_axis=0, tiled=True)  13.4 us
    all_to_all x1, waiting for transfers between devices, shards(): lax.all_to_all(value_local, 'sp', split_axis=1, concat_axis=0, tiled=True)  12.4 us
  transfers between devices with their start and end apart: 7, of which 6 were waited for; matrix products, arithmetic and copies ran while one was open for 27% of the time, Pallas kernels for 0%

profile of v1, /device:TPU:0, one launch (start us, length us, event | category | flops | bytes accessed | tf_op | source)
XLA Modules:
  0.0 361.9 jit_solution(1728737718007709858)
XLA Ops:
  8.6 7.3 %all-to-all-start.1 = ((bf16[128,16,128]{0,2,1:T(8,128)(2,1)}), bf16[128,16,128]{0,2,1:T(8,128)(2,1)S(1)}, u32[]{:S(2)}, u32[]{:S(2)}) async-start(bf16[128,16,128]{0,2,1:T(8,128)(2,1)} %bitcast.6), calls=%async_computation.1 | async-start | bytes 1048576 | tf_op jit(solution)/shard_map/all_to_all | solution.py:84
  16.9 13.4 %all-to-all-done.1 = bf16[128,16,128]{0,2,1:T(8,128)(2,1)S(1)} async-done(((bf16[128,16,128]{0,2,1:T(8,128)(2,1)}), bf16[128,16,128]{0,2,1:T(8,128)(2,1)S(1)}, u32[]{:S(2)}, u32[]{:S(2)}) %all-to-all-start.1) | async-done | bytes 524320 | tf_op jit(solution)/shard_map/all_to_all | solution.py:84
  30.3 3.6 %all-to-all-start.2 = ((bf16[128,16,128]{0,2,1:T(8,128)(2,1)}), bf16[128,16,128]{0,2,1:T(8,128)(2,1)S(1)}, u32[]{:S(2)}, u32[]{:S(2)}) async-start(bf16[128,16,128]{0,2,1:T(8,128)(2,1)} %bitcast.13), calls=%async_computation.2 | async-start | bytes 1048576 | tf_op jit(solution)/shard_map/all_to_all | solution.py:82
  35.0 13.7 %all-to-all-done.2 = bf16[128,16,128]{0,2,1:T(8,128)(2,1)S(1)} async-done(((bf16[128,16,128]{0,2,1:T(8,128)(2,1)}), bf16[128,16,128]{0,2,1:T(8,128)(2,1)S(1)}, u32[]{:S(2)}, u32[]{:S(2)}) %all-to-all-start.2) | async-done | bytes 524320 | tf_op jit(solution)/shard_map/all_to_all | solution.py:82
  48.7 4.2 %all-to-all-start = ((bf16[128,16,128]{0,2,1:T(8,128)(2,1)}), bf16[128,16,128]{0,2,1:T(8,128)(2,1)}, u32[]{:S(2)}, u32[]{:S(2)}) async-start(bf16[128,16,128]{0,2,1:T(8,128)(2,1)} %bitcast.1), calls=%async_computation | async-start | bytes 1048576 | tf_op jit(solution)/shard_map/all_to_all | solution.py:81
  56.1 11.0 %all-to-all-done = bf16[128,16,128]{0,2,1:T(8,128)(2,1)} async-done(((bf16[128,16,128]{0,2,1:T(8,128)(2,1)}), bf16[128,16,128]{0,2,1:T(8,128)(2,1)}, u32[]{:S(2)}, u32[]{:S(2)}) %all-to-all-start) | async-done | bytes 524320 | tf_op jit(solution)/shard_map/all_to_all | solution.py:81
  67.1 3.7 %all-to-all-start.3 = ((bf16[128,16,256]{0,2,1:T(8,128)(2,1)}), bf16[128,16,256]{0,2,1:T(8,128)(2,1)S(1)}, u32[]{:S(2)}, u32[]{:S(2)}) async-start(bf16[128,16,256]{0,2,1:T(8,128)(2,1)} %bitcast.18), calls=%async_computation.3 | async-start | bytes 2097152 | tf_op jit(solution)/shard_map/all_to_all | solution.py:83
  76.7 4.0 %exponential_multiply_fusion = (f32[16,64,2,128]{3,0,1,2:T(8,128)}, f32[16,64,2,128]{3,0,1,2:T(8,128)S(1)}, f32[16,64,2,128]{3,0,1,2:T(8,128)S(1)}) fusion(f32[16,64,2,128]{3,0,1,2:T(8,128)S(1)} %fusion.30, f32[16,64,2,128]{3,1,0,2:T(8,128)} %bitcast.136, f32[16,2,128]{2,0,1:T(8,128)S(1)} %slice_bitcast_fusion.8, f32[16,64,2,128]{3,1,0,2:T(8,128)} %bitcast.137), kind=kLoop, calls=%fused_computation.49 | loop fusion | flops 1310720 | bytes 6307840 | tf_op jit(solution)/shard_map/mul | solution.py:41
  80.7 3.5 convolution_select_fusion
  84.2 12.4 %all-to-all-done.3 = bf16[128,16,256]{0,2,1:T(8,128)(2,1)S(1)} async-done(((bf16[128,16,256]{0,2,1:T(8,128)(2,1)}), bf16[128,16,256]{0,2,1:T(8,128)(2,1)S(1)}, u32[]{:S(2)}, u32[]{:S(2)}) %all-to-all-start.3) | async-done | bytes 1048608 | tf_op jit(solution)/shard_map/all_to_all | solution.py:83
  97.1 3.7 %fusion.27 = f32[16,2,128,256]{3,2,1,0:T(8,128)S(1)} fusion(f32[16,64,2,128]{3,0,1,2:T(8,128)} %get-tuple-element.7, bf16[16,64,2,256]{3,1,0,2:T(8,128)(2,1)S(1)} %bitcast.127), kind=kOutput, calls=%fused_computation.40 | convolution fusion | flops 805306368 | bytes 6291456 | tf_op jit(solution)/shard_map/nshk,nshv->nhkv/dot_general | solution.py:42
  106.4 4.2 %pad.30 = f32[4,2,128,256]{3,2,1,0:T(8,128)} pad(f32[2,2,128,256]{3,2,1,0:T(8,128)} %pad_add_fusion, f32[]{:T(128)} %constant.27.clone.1), padding=1_0_1x0_0_0x0_0_0x0_0_0 | pad | bytes 1572868 | tf_op jit(solution)/shard_map/pad | solution.py:44
  112.6 4.1 %pad.29 = f32[4,2,128,256]{3,2,1,0:T(8,128)} pad(f32[2,2,128,256]{3,2,1,0:T(8,128)} %pad_maximum_fusion.2, f32[]{:T(128)} %constant.27.clone.1), padding=0_1_1x0_0_0x0_0_0x0_0_0 | pad | bytes 1572868 | tf_op jit(solution)/shard_map/pad | solution.py:44
  116.7 2.8 add.160
  121.5 3.9 %pad.31 = f32[8,2,128,256]{3,2,1,0:T(8,128)S(1)} pad(f32[4,2,128,256]{3,2,1,0:T(8,128)} %pad_maximum_fusion.1, f32[]{:T(128)} %constant.27.clone.1), padding=0_1_1x0_0_0x0_0_0x0_0_0 | pad | bytes 3145732 | tf_op jit(solution)/shard_map/pad | solution.py:44
  125.4 6.6 %pad.32 = f32[8,2,128,256]{3,2,1,0:T(8,128)} pad(f32[4,2,128,256]{3,2,1,0:T(8,128)} %add.160, f32[]{:T(128)} %constant.27.clone.1), padding=1_0_1x0_0_0x0_0_0x0_0_0 | pad | bytes 3145732 | tf_op jit(solution)/shard_map/pad | solution.py:44
  132.0 3.2 add.162
  135.2 11.5 %pad.66 = f32[16,2,128,256]{3,2,1,0:T(8,128)} pad(f32[8,2,128,256]{3,2,1,0:T(8,128)} %add.162, f32[]{:T(128)} %constant.27.clone.1), padding=1_0_1x0_0_0x0_0_0x0_0_0 | pad | bytes 6291460
  150.6 11.5 %pad.44 = f32[15,2,128,256]{3,2,1,0:T(8,128)} pad(f32[8,2,128,256]{3,2,1,0:T(8,128)} %pad_maximum_fusion, f32[]{:T(128)} %constant.27.clone.1), padding=0_0_1x0_0_0x0_0_0x0_0_0 | pad | bytes 6029316 | tf_op jit(solution)/shard_map/slice | solution.py:45
  164.3 2.9 fusion.16.clone.4
  167.2 2.9 multiply_reduce_fusion.1
  175.9 3.6 %all-to-all-start.4 = ((bf16[8,128,2,256]{3,1,2,0:T(8,128)(2,1)}), bf16[8,128,2,256]{3,1,2,0:T(8,128)(2,1)S(1)}, u32[]{:S(2)}, u32[]{:S(2)}) async-start(bf16[8,128,2,256]{3,1,2,0:T(8,128)(2,1)} %fusion.44), calls=%async_computation.4 | async-start | bytes 2097152 | tf_op jit(solution)/shard_map/all_to_all | solution.py:102
  182.6 22.9 %all-to-all-done.4 = bf16[8,128,2,256]{3,1,2,0:T(8,128)(2,1)S(1)} async-done(((bf16[8,128,2,256]{3,1,2,0:T(8,128)(2,1)}), bf16[8,128,2,256]{3,1,2,0:T(8,128)(2,1)S(1)}, u32[]{:S(2)}, u32[]{:S(2)}) %all-to-all-start.4) | async-done | bytes 1048608 | tf_op jit(solution)/shard_map/all_to_all | solution.py:102
  206.3 8.3 %multiply_reduce_fusion.3 = (f32[128]{0:T(128)S(1)}, f32[128,2048]{1,0:T(8,128)S(1)}) fusion(bf16[128,4096]{0,1:T(8,128)(2,1)S(1)} %bitcast.129, bf16[4096,2048]{1,0:T(8,128)(2,1)} %all-gather.2.cloned.1.call-done), kind=kOutput, calls=%fused_computation.47 | convolution fusion | flops 2148532224 | bytes 18874880 | tf_op jit(solution)/shard_map/dot_general | solution.py:106
  215.5 3.2 gather_fusion
  220.4 52.3 %all_to_all.57 = bf16[32,13,2048]{2,1,0:T(8,128)(2,1)} all-to-all(bf16[32,13,2048]{2,1,0:T(8,128)(2,1)S(1)} %reshape.175), channel_id=1, replica_groups=mesh['sp'=8,'dp'=4] {'sp','dp'}, dimensions={0} | all-to-all | bytes 3407872 | tf_op jit(solution)/shard_map/all_to_all | solution.py:131
  274.6 5.3 %fusion.4 = f32[416,1024]{1,0:T(8,128)} fusion(bf16[416,2048]{1,0:T(8,128)(2,1)S(1)} %reshape.176, bf16[1,2048,1024]{2,1,0:T(8,128)(2,1)} %param.26), kind=kOutput, calls=%fused_computation.7 | convolution fusion | flops 1744830464 | bytes 7602176 | tf_op jit(solution)/shard_map/dot_general | solution.py:133
  279.9 8.9 %fusion.8 = bf16[416,2048]{1,0:T(8,128)(2,1)} fusion(bf16[1,1024,2048]{2,1,0:T(8,128)(2,1)} %param.28, f32[416,1024]{1,0:T(8,128)} %fusion.4, bf16[416,2048]{1,0:T(8,128)(2,1)S(1)} %reshape.176, bf16[1,2048,1024]{2,1,0:T(8,128)(2,1)} %param.27), kind=kOutput, calls=%fused_computation.12 | convolution fusion | flops 3493068800 | bytes 13500416 | tf_op jit(solution)/shard_map/dot_general | solution.py:136
  288.8 2.8 reshape.177
  291.6 3.8 %all-to-all-start.6 = ((bf16[32,13,2048]{2,1,0:T(8,128)(2,1)}), bf16[32,13,2048]{2,1,0:T(8,128)(2,1)}, u32[]{:S(2)}, u32[]{:S(2)}) async-start(bf16[32,13,2048]{2,1,0:T(8,128)(2,1)} %reshape.177), calls=%async_computation.6 | async-start | bytes 4194304 | tf_op jit(solution)/shard_map/all_to_all | solution.py:139
  295.5 48.5 %all-to-all-done.6 = bf16[32,13,2048]{2,1,0:T(8,128)(2,1)} async-done(((bf16[32,13,2048]{2,1,0:T(8,128)(2,1)}), bf16[32,13,2048]{2,1,0:T(8,128)(2,1)}, u32[]{:S(2)}, u32[]{:S(2)}) %all-to-all-start.6) | async-done | bytes 1703968 | tf_op jit(solution)/shard_map/all_to_all | solution.py:139
  350.6 3.2 multiply_reduce_fusion
  (145 shorter events, 51.3 us)
Async XLA Ops:
  6.5 1.0 copy-start.12
  6.5 199.7 %all-gather.2.cloned.1.call-start = ((), (), s32[]{:S(2)}) async-start(), calls=%async_computation.7 | async-start | bytes 20971520 | tf_op jit(solution)/shard_map/all_gather | solution.py:108
  7.6 8.3 %copy-start.13 = (bf16[1,128,2048]{2,1,0:T(8,128)(2,1)S(1)}, bf16[1,128,2048]{2,1,0:T(8,128)(2,1)}, u32[]{:S(2)}) copy-start(bf16[1,128,2048]{2,1,0:T(8,128)(2,1)} %param.18) | copy-start | bytes 1572868
  7.6 26.4 %copy-start.14 = (bf16[1,128,2048]{2,1,0:T(8,128)(2,1)S(1)}, bf16[1,128,2048]{2,1,0:T(8,128)(2,1)}, u32[]{:S(2)}) copy-start(bf16[1,128,2048]{2,1,0:T(8,128)(2,1)} %param.17) | copy-start | bytes 1572868
  8.6 21.8 %all-to-all-start.1 = ((bf16[128,16,128]{0,2,1:T(8,128)(2,1)}), bf16[128,16,128]{0,2,1:T(8,128)(2,1)S(1)}, u32[]{:S(2)}, u32[]{:S(2)}) async-start(bf16[128,16,128]{0,2,1:T(8,128)(2,1)} %bitcast.6), calls=%async_computation.1 | async-start | bytes 1048576 | tf_op jit(solution)/shard_map/all_to_all | solution.py:84
  15.9 37.0 %copy-start.19 = (f32[1,2,1024]{2,1,0:T(2,128)S(1)}, f32[1,2,1024]{2,1,0:T(2,128)}, u32[]{:S(2)}) copy-start(f32[1,2,1024]{2,1,0:T(2,128)} %param.21) | copy-start | bytes 24580
  15.9 37.0 %copy-start.10 = (bf16[1,128,4096]{2,1,0:T(8,128)(2,1)S(1)}, bf16[1,128,4096]{2,1,0:T(8,128)(2,1)}, u32[]{:S(2)}) copy-start(bf16[1,128,4096]{2,1,0:T(8,128)(2,1)} %param.19) | copy-start | bytes 3145732
  30.3 18.3 %all-to-all-start.2 = ((bf16[128,16,128]{0,2,1:T(8,128)(2,1)}), bf16[128,16,128]{0,2,1:T(8,128)(2,1)S(1)}, u32[]{:S(2)}, u32[]{:S(2)}) async-start(bf16[128,16,128]{0,2,1:T(8,128)(2,1)} %bitcast.13), calls=%async_computation.2 | async-start | bytes 1048576 | tf_op jit(solution)/shard_map/all_to_all | solution.py:82
  48.7 6.5 %copy-start.9 = (bf16[128,16,128]{0,2,1:T(8,128)(2,1)}, bf16[128,16,128]{0,2,1:T(8,128)(2,1)S(1)}, u32[]{:S(2)}) copy-start(bf16[128,16,128]{0,2,1:T(8,128)(2,1)S(1)} %all-to-all-done.2) | copy-start | bytes 1572868
  48.7 18.4 %all-to-all-start = ((bf16[128,16,128]{0,2,1:T(8,128)(2,1)}), bf16[128,16,128]{0,2,1:T(8,128)(2,1)}, u32[]{:S(2)}, u32[]{:S(2)}) async-start(bf16[128,16,128]{0,2,1:T(8,128)(2,1)} %bitcast.1), calls=%async_computation | async-start | bytes 1048576 | tf_op jit(solution)/shard_map/all_to_all | solution.py:81
  67.1 29.5 %all-to-all-start.3 = ((bf16[128,16,256]{0,2,1:T(8,128)(2,1)}), bf16[128,16,256]{0,2,1:T(8,128)(2,1)S(1)}, u32[]{:S(2)}, u32[]{:S(2)}) async-start(bf16[128,16,256]{0,2,1:T(8,128)(2,1)} %bitcast.18), calls=%async_computation.3 | async-start | bytes 2097152 | tf_op jit(solution)/shard_map/all_to_all | solution.py:83
  97.1 3.7 %copy-start.2 = (bf16[8,128,2,256]{3,1,0,2:T(8,128)(2,1)}, bf16[8,128,2,256]{3,1,0,2:T(8,128)(2,1)S(1)}, u32[]{:S(2)}) copy-start(bf16[8,128,2,256]{3,1,0,2:T(8,128)(2,1)S(1)} %copy.191) | copy-start | bytes 3145732
  100.8 1.9 copy-start
  103.7 1.0 copy-start.6
  104.9 0.7 copy-start.8
  116.7 2.8 copy-start.4
  116.7 2.8 copy-start.5
  119.5 1.0 copy-start.11
  146.6 2.5 slice-start
  150.6 11.5 %copy-start.3 = (bf16[8,128,2,256]{3,1,0,2:T(8,128)(2,1)S(1)}, bf16[8,128,2,256]{3,1,0,2:T(8,128)(2,1)}, u32[]{:S(2)}) copy-start(bf16[8,128,2,256]{3,1,0,2:T(8,128)(2,1)} %copy-done.2) | copy-start | bytes 3145732
  150.6 11.5 %copy-start.7 = (f32[16,2,64,64]{3,2,1,0:T(8,128)S(1)}, f32[16,2,64,64]{3,2,1,0:T(8,128)}, u32[]{:S(2)}) copy-start(f32[16,2,64,64]{3,2,1,0:T(8,128)} %convolution_select_fusion) | copy-start | bytes 1572868
  162.1 2.2 copy-start.1
  170.7 8.9 %copy-start.20 = (s32[1,128,2]{1,2,0:T(2,128)S(1)}, s32[1,128,2]{1,2,0:T(2,128)}, u32[]{:S(2)}) copy-start(s32[1,128,2]{1,2,0:T(2,128)} %param.30) | copy-start | bytes 3076
  175.9 29.6 %all-to-all-start.4 = ((bf16[8,128,2,256]{3,1,2,0:T(8,128)(2,1)}), bf16[8,128,2,256]{3,1,2,0:T(8,128)(2,1)S(1)}, u32[]{:S(2)}, u32[]{:S(2)}) async-start(bf16[8,128,2,256]{3,1,2,0:T(8,128)(2,1)} %fusion.44), calls=%async_computation.4 | async-start | bytes 2097152 | tf_op jit(solution)/shard_map/all_to_all | solution.py:102
  206.2 8.3 %copy-start.15 = (bf16[1,128,2048]{2,1,0:T(8,128)(2,1)S(1)}, bf16[1,128,2048]{2,1,0:T(8,128)(2,1)}, u32[]{:S(2)}) copy-start(bf16[1,128,2048]{2,1,0:T(8,128)(2,1)} %param.16) | copy-start | bytes 1572868
  206.2 8.3 %copy-start.16 = (f32[2048]{0:T(1024)S(1)}, f32[2048]{0:T(1024)}, u32[]{:S(2)}) copy-start(f32[2048]{0:T(1024)} %param.24) | copy-start | bytes 24580
  214.5 0.7 copy-start.17
  291.6 3.8 %copy-start.21 = (f32[1,128,2]{1,2,0:T(2,128)S(1)}, f32[1,128,2]{1,2,0:T(2,128)}, u32[]{:S(2)}) copy-start(f32[1,128,2]{1,2,0:T(2,128)} %param.31) | copy-start | bytes 3076
  291.6 52.5 %all-to-all-start.6 = ((bf16[32,13,2048]{2,1,0:T(8,128)(2,1)}), bf16[32,13,2048]{2,1,0:T(8,128)(2,1)}, u32[]{:S(2)}, u32[]{:S(2)}) async-start(bf16[32,13,2048]{2,1,0:T(8,128)(2,1)} %reshape.177), calls=%async_computation.6 | async-start | bytes 4194304 | tf_op jit(solution)/shard_map/all_to_all | solution.py:139
  350.6 3.3 copy-start.18
Sparse Core Ops, SparseCore 0:
  8.9 108.6 all-gather.1
